TPU v7x, 32 devices: a whole 2x2x4 slice. The times are simulated.
32 devices in a mesh: sp: 16 (over z, y, x), tp: 2 (over core).
Axes of the slice: x: 2, y: 2, z: 4, core: 2. Of those that a mesh axis runs over, the one named last changes fastest.
Arguments:
- stream: bfloat16 [6144, 2048], P('sp', 'tp'), may hold values from -6 to 6
- norm_gain: float32 [2, 2048], replicated, may hold values from 0.1 to 1.9
- a_weight: bfloat16 [2, 2048, 2048], P(None, 'sp', 'tp'), may hold values from -0.125 to 0.125
- gate_weight: bfloat16 [2, 2048, 2048], P(None, 'sp', 'tp'), may hold values from -0.125 to 0.125
- conv_weight: float32 [2, 31, 2048], P(None, None, 'tp'), may hold values from -4 to 4, as said below
- conv_bias: float32 [2, 2048], P(None, 'tp'), may hold values from -3 to 3
- ln_gain: float32 [2, 2048], P(None, 'tp'), may hold values from 0.1 to 1.9
- ln_shift: float32 [2, 2048], P(None, 'tp'), may hold values from -3 to 3
- out_weight: bfloat16 [2, 2048, 2048], P(None, 'sp', 'tp'), may hold values from -0.125 to 0.125
Outputs:
- result: bfloat16 [6144, 2048], P('sp', 'tp')
Inputs may be any that keep to these rules, and one draw needn't show every extreme that they name: `conv_weight`: each column is drawn with its own scale, and blocks of 16 channels differ in scale by up to a factor of nine.
All inputs are finite; a program needn't handle non-finite values.
Results may differ from a plain program's by a relative error of at most 0.01.
Values may be sent and summed in bfloat16 or wider, within the bound.
A program may use at most 64 MiB of HBM per device.

v0:
```python
import jax
import jax.numpy as jnp
from jax import lax
from jax.sharding import PartitionSpec as P

D = 2048


EPSILON = 1e-06


def with_halo(block, sides, width):
    for axis, dim in sides:
        count = lax.axis_size(axis)
        forward = [(i, i + 1) for i in range(count - 1)]
        backward = [(target, source) for source, target in forward]
        low = lax.ppermute(
            lax.slice_in_dim(block, block.shape[dim] - width, None, axis=dim), axis, forward
        )
        high = lax.ppermute(lax.slice_in_dim(block, 0, width, axis=dim), axis, backward)
        block = jnp.concatenate([low, block, high], axis=dim)
    return block


def normalize_rows(stream_f, gain):
    factor = lax.rsqrt(jnp.mean(stream_f * stream_f, axis=1, keepdims=True) + EPSILON)
    return (stream_f * factor * gain[None, :]).astype(jnp.bfloat16)


def convolve(padded, kernel, conv_shift, out_rows):
    summed = jnp.zeros((out_rows, padded.shape[1]), jnp.float32) + conv_shift[None, :]
    for offset in range(kernel.shape[0]):
        window = lax.slice_in_dim(padded, offset, offset + out_rows, axis=0).astype(jnp.float32)
        summed = summed + window * kernel[offset][None, :]
    return summed


def finish_norm(conv_out, row_sum, row_squares, gain, shift):
    average = row_sum / D
    variance = row_squares / D - average * average
    normed = (conv_out - average) * lax.rsqrt(variance + EPSILON) * gain[None, :] + shift[None, :]
    return jax.nn.silu(normed).astype(jnp.bfloat16)


def local(
    stream, norm_gain, a_weight, gate_weight, conv_weight, conv_bias, ln_gain, ln_shift, out_weight
):
    reach = (conv_weight.shape[1] - 1) // 2
    layer_total = a_weight.shape[0]
    gathered = (
        lax.all_gather(a_weight, "sp", axis=1, tiled=True),
        lax.all_gather(gate_weight, "sp", axis=1, tiled=True),
        lax.all_gather(out_weight, "sp", axis=1, tiled=True),
    )
    current = stream
    for layer_index in range(layer_total):
        stream_f = current.astype(jnp.float32)
        full_rows = lax.all_gather(current, "tp", axis=1, tiled=True)
        normed = normalize_rows(full_rows.astype(jnp.float32), norm_gain[layer_index])
        linear = jnp.dot(normed, gathered[0][layer_index], preferred_element_type=jnp.float32)
        gating = jnp.dot(normed, gathered[1][layer_index], preferred_element_type=jnp.float32)
        product = linear * jax.nn.sigmoid(gating)
        gated = product.astype(jnp.bfloat16)
        padded = with_halo(gated, (("sp", 0),), reach)
        out_rows = padded.shape[0] - 2 * reach
        conv_out = convolve(padded, conv_weight[layer_index], conv_bias[layer_index], out_rows)
        row_sum, row_squares = lax.psum(
            (
                jnp.sum(conv_out, axis=1, keepdims=True),
                jnp.sum(conv_out * conv_out, axis=1, keepdims=True),
            ),
            "tp",
        )
        mixed_in = finish_norm(
            conv_out, row_sum, row_squares, ln_gain[layer_index], ln_shift[layer_index]
        )
        mixed_rows = lax.all_gather(mixed_in, "tp", axis=1, tiled=True)
        branch = jnp.dot(mixed_rows, gathered[2][layer_index], preferred_element_type=jnp.float32)
        current = (stream_f + branch).astype(jnp.bfloat16)
    return current


def solution(mesh):
    placed = (
        P("sp", "tp"),
        P(),
        P(None, "sp", "tp"),
        P(None, "sp", "tp"),
        P(None, None, "tp"),
        P(None, "tp"),
        P(None, "tp"),
        P(None, "tp"),
        P(None, "sp", "tp"),
    )
    return jax.shard_map(
        local, mesh=mesh, in_specs=placed, out_specs=P("sp", "tp"), check_vma=False
    )
```

profile of v0, /device:TPU:9, one launch (start us, length us, event | category | flops | bytes accessed | tf_op | source)
XLA Modules:
  0.0 443.0 jit_solution(733793492786073124)
XLA Ops:
  9.7 10.9 %all-gather.8.cloned.1.call-done = bf16[384,2048]{1,0:T(8,128)(2,1)} async-done(((bf16[384,1024]{1,0:T(8,128)(2,1)}), bf16[384,2048]{1,0:T(8,128)(2,1)}) %all-gather.8.cloned.1.call-update) | async-done | bytes 1572880 | tf_op jit(solution)/shard_map/all_gather | solution.py:58
  20.6 1.9 fusion.6
  22.5 110.7 %all-gather.12.cloned.1.call-done = bf16[2,2048,1024]{2,1,0:T(8,128)(2,1)} async-done(((bf16[2,128,1024]{2,1,0:T(8,128)(2,1)}), bf16[2,2048,1024]{2,1,0:T(8,128)(2,1)}) %all-gather.12.cloned.1.call-update) | async-done | bytes 8388624 | tf_op jit(solution)/shard_map/all_gather | solution.py:52
  133.2 5.3 %fusion.4 = f32[384,1024]{1,0:T(8,128)} fusion(bf16[2,2048,1024]{2,1,0:T(8,128)(2,1)} %all-gather.12.cloned.1.call-done, bf16[384,2048]{1,0:T(8,128)(2,1)S(1)} %copy-done, f32[2048]{0:T(1024)S(1)} %bitcast.168, f32[384]{0:T(512)S(1)} %add_rsqrt_fusion.1), kind=kOutput, calls=%fused_computation.65 | convolution fusion | flops 1613758464 | bytes 7349760 | tf_op jit(solution)/shard_map/dot_general | solution.py:61
  138.5 107.9 %all-gather.10.cloned.1.call-done = bf16[2,2048,1024]{2,1,0:T(8,128)(2,1)} async-done(((bf16[2,128,1024]{2,1,0:T(8,128)(2,1)}), bf16[2,2048,1024]{2,1,0:T(8,128)(2,1)}) %all-gather.10.cloned.1.call-update) | async-done | bytes 8388624 | tf_op jit(solution)/shard_map/all_gather | solution.py:51
  246.4 4.6 %multiply_convert_fusion.3 = bf16[384,1024]{1,0:T(8,128)(2,1)S(1)} fusion(f32[384,1024]{1,0:T(8,128)} %fusion.4, bf16[2,2048,1024]{2,1,0:T(8,128)(2,1)} %all-gather.10.cloned.1.call-done, bf16[384,2048]{1,0:T(8,128)(2,1)S(1)} %copy-done, f32[2048]{0:T(1024)S(1)} %bitcast.169, f32[384]{0:T(512)S(1)} %add_rsqrt_fusion.1), kind=kOutput, calls=%fused_computation.87 | convolution fusion | flops 1615724544 | bytes 8136192 | tf_op jit(solution)/shard_map/dot_general | solution.py:60
  251.0 4.3 collective-permute-start.1
  255.3 1.9 collective-permute-start
  257.3 4.5 %collective-permute-done = bf16[15,1024]{1,0:T(8,128)(2,1)S(1)} collective-permute-done((bf16[15,1024]{1,0:T(8,128)(2,1)S(1)}, bf16[15,1024]{1,0:T(8,128)(2,1)S(1)}, u32[]{:S(2)}, u32[]{:S(2)}) %collective-permute-start) | collective-permute-done | bytes 30752 | tf_op jit(solution)/shard_map/ppermute | solution.py:17
  261.8 8.1 %fusion.73 = (f32[384]{0:T(512)S(1)}, f32[384]{0:T(512)S(1)}, f32[384,1024]{1,0:T(8,128)S(1)}) fusion(f32[1024]{0:T(1024)S(1)} %bitcast.114, bf16[15,1024]{1,0:T(8,128)(2,1)S(1)} %collective-permute-done.1, bf16[384,1024]{1,0:T(8,128)(2,1)S(1)} %multiply_convert_fusion.3, f32[1024]{0:T(1024)S(1)} %bitcast.115, f32[1024]{0:T(1024)S(1)} %bitcast.116, ...), kind=kLoop, calls=%fused_computation.189 | loop fusion | flops 73137408 | bytes 2554880 | tf_op jit(solution)/shard_map/reduce_sum | solution.py:69
  269.9 6.6 %all-reduce.1 = (f32[384,1]{0,1:T(1,128)S(1)}, f32[384,1]{0,1:T(1,128)S(1)}) all-reduce(f32[384,1]{0,1:T(1,128)S(1)} %broadcast_in_dim.14, f32[384,1]{0,1:T(1,128)S(1)} %broadcast_in_dim.15), channel_id=1, replica_groups=mesh['sp'=16,'tp'=2] {'tp'}, use_global_device_ids=true, to_apply=%region_2.0 | all-reduce | flops 768 | bytes 6144 | tf_op jit(solution)/shard_map/psum | solution.py:67
  278.1 81.3 %all-gather.16.cloned.1.call-done = bf16[2,2048,1024]{2,1,0:T(8,128)(2,1)} async-done(((bf16[2,128,1024]{2,1,0:T(8,128)(2,1)}), bf16[2,2048,1024]{2,1,0:T(8,128)(2,1)}) %all-gather.16.cloned.1.call-update) | async-done | bytes 8388624 | tf_op jit(solution)/shard_map/all_gather | solution.py:53
  359.4 12.9 %all-gather.14.cloned.1.call-done = bf16[384,2048]{1,0:T(8,128)(2,1)} async-done(((bf16[384,1024]{1,0:T(8,128)(2,1)}), bf16[384,2048]{1,0:T(8,128)(2,1)}) %all-gather.14.cloned.1.call-update) | async-done | bytes 1572880 | tf_op jit(solution)/shard_map/all_gather | solution.py:77
  372.4 5.3 %add_convert_fusion.1 = bf16[384,1024]{1,0:T(8,128)(2,1)} fusion(bf16[384,1024]{1,0:T(8,128)(2,1)S(1)} %copy-done.2, bf16[384,2048]{1,0:T(8,128)(2,1)} %all-gather.14.cloned.1.call-done, bf16[2,2048,1024]{2,1,0:T(8,128)(2,1)} %all-gather.16.cloned.1.call-done), kind=kOutput, calls=%fused_computation.83 | convolution fusion | flops 1611792384 | bytes 7340032 | tf_op jit(solution)/shard_map/dot_general | solution.py:78
  377.8 11.1 %all-gather.18.cloned.1.call-done = bf16[384,2048]{1,0:T(8,128)(2,1)} async-done(((bf16[384,1024]{1,0:T(8,128)(2,1)}), bf16[384,2048]{1,0:T(8,128)(2,1)}) %all-gather.18.cloned.1.call-update) | async-done | bytes 1572880 | tf_op jit(solution)/shard_map/all_gather | solution.py:58
  390.8 4.2 fusion.1
  395.5 1.9 multiply_convert_fusion.1
  397.4 4.0 collective-permute-start.3
  401.4 1.9 collective-permute-start.2
  403.4 4.4 collective-permute-done.2
  407.9 8.1 %fusion.72 = (f32[384]{0:T(512)S(1)}, f32[384]{0:T(512)S(1)}, f32[384,1024]{1,0:T(8,128)S(1)}) fusion(f32[1024]{0:T(1024)S(1)} %bitcast.98, bf16[15,1024]{1,0:T(8,128)(2,1)S(1)} %collective-permute-done.3, bf16[384,1024]{1,0:T(8,128)(2,1)S(1)} %multiply_convert_fusion.1, f32[1024]{0:T(1024)S(1)} %bitcast.109, f32[1024]{0:T(1024)S(1)} %bitcast.142, ...), kind=kLoop, calls=%fused_computation.188 | loop fusion | flops 73137408 | bytes 2554880 | tf_op jit(solution)/shard_map/reduce_sum | solution.py:69
  416.0 3.8 all-reduce
  421.3 9.4 %all-gather.20.cloned.1.call-done = bf16[384,2048]{1,0:T(8,128)(2,1)} async-done(((bf16[384,1024]{1,0:T(8,128)(2,1)}), bf16[384,2048]{1,0:T(8,128)(2,1)}) %all-gather.20.cloned.1.call-update) | async-done | bytes 1572880 | tf_op jit(solution)/shard_map/all_gather | solution.py:77
  430.8 5.3 %add_convert_fusion = bf16[384,1024]{1,0:T(8,128)(2,1)} fusion(bf16[384,1024]{1,0:T(8,128)(2,1)S(1)} %copy-done.3, bf16[384,2048]{1,0:T(8,128)(2,1)} %all-gather.20.cloned.1.call-done, bf16[2,2048,1024]{2,1,0:T(8,128)(2,1)} %all-gather.16.cloned.1.call-done), kind=kOutput, calls=%fused_computation.78 | convolution fusion | flops 1611792384 | bytes 7340032 | tf_op jit(solution)/shard_map/dot_general | solution.py:78
  (57 shorter events, 8.7 us)
Async XLA Ops:
  6.5 2.8 copy-start.6
  6.5 2.9 copy-start.7
  6.5 2.9 copy-start.4
  6.5 3.1 copy-start.5
  6.5 14.1 %all-gather.8.cloned.1.call-start = ((), (), s32[]{:S(2)}) async-start(), calls=%async_computation | async-start | bytes 2359296 | tf_op jit(solution)/shard_map/all_gather | solution.py:58
  7.3 126.0 %all-gather.12.cloned.1.call-start = ((), (), s32[]{:S(2)}) async-start(), calls=%async_computation.2 | async-start | bytes 8912896 | tf_op jit(solution)/shard_map/all_gather | solution.py:52
  8.0 238.4 %all-gather.10.cloned.1.call-start = ((), (), s32[]{:S(2)}) async-start(), calls=%async_computation.1 | async-start | bytes 8912896 | tf_op jit(solution)/shard_map/all_gather | solution.py:51
  8.8 350.7 %all-gather.16.cloned.1.call-start = ((), (), s32[]{:S(2)}) async-start(), calls=%async_computation.4 | async-start | bytes 8912896 | tf_op jit(solution)/shard_map/all_gather | solution.py:53
  9.3 363.0 %all-gather.14.cloned.1.call-start = ((), (), s32[]{:S(2)}) async-start(), calls=%async_computation.3 | async-start | bytes 2359296 | tf_op jit(solution)/shard_map/all_gather | solution.py:77
  20.6 112.6 %copy-start = (bf16[384,2048]{1,0:T(8,128)(2,1)S(1)}, bf16[384,2048]{1,0:T(8,128)(2,1)}, u32[]{:S(2)}) copy-start(bf16[384,2048]{1,0:T(8,128)(2,1)} %all-gather.8.cloned.1.call-done) | copy-start | bytes 4718596
  138.5 118.8 %copy-start.8 = (f32[2,1024]{1,0:T(2,128)S(1)}, f32[2,1024]{1,0:T(2,128)}, u32[]{:S(2)}) copy-start(f32[2,1024]{1,0:T(2,128)} %param.15) | copy-start | bytes 24580
  251.0 6.2 %collective-permute-start.1 = (bf16[15,1024]{1,0:T(8,128)(2,1)S(1)}, bf16[15,1024]{1,0:T(8,128)(2,1)S(1)}, u32[]{:S(2)}, u32[]{:S(2)}) collective-permute-start(bf16[15,1024]{1,0:T(8,128)(2,1)S(1)} %get-tuple-element.22), channel_id=1, source_target_pairs={{2,0},{4,2},{6,4},{8,6},{10,8},{12,10},{14,12},{16,14},{18,16},{20... | collective-permute-start | bytes 92168 | tf_op jit(solution)/shard_map/ppermute | solution.py:20
  255.3 6.5 %collective-permute-start = (bf16[15,1024]{1,0:T(8,128)(2,1)S(1)}, bf16[15,1024]{1,0:T(8,128)(2,1)S(1)}, u32[]{:S(2)}, u32[]{:S(2)}) collective-permute-start(bf16[15,1024]{1,0:T(8,128)(2,1)S(1)} %get-tuple-element.21), channel_id=1, source_target_pairs={{0,2},{2,4},{4,6},{6,8},{8,10},{10,12},{12,14},{14,16},{16,18},{18... | collective-permute-start | bytes 92168 | tf_op jit(solution)/shard_map/ppermute | solution.py:17
  276.5 95.8 %copy-start.2 = (bf16[384,1024]{1,0:T(8,128)(2,1)S(1)}, bf16[384,1024]{1,0:T(8,128)(2,1)}, u32[]{:S(2)}) copy-start(bf16[384,1024]{1,0:T(8,128)(2,1)} %param.9) | copy-start | bytes 2359300
  278.1 110.8 %all-gather.18.cloned.1.call-start = ((), (), s32[]{:S(2)}) async-start(), calls=%async_computation.5 | async-start | bytes 2359296 | tf_op jit(solution)/shard_map/all_gather | solution.py:58
  377.7 53.0 %all-gather.20.cloned.1.call-start = ((), (), s32[]{:S(2)}) async-start(), calls=%async_computation.6 | async-start | bytes 2359296 | tf_op jit(solution)/shard_map/all_gather | solution.py:77
  388.9 1.9 copy-start.1
  390.8 4.6 %copy-start.9 = (bf16[2,2048,1024]{2,1,0:T(8,128)(2,1)S(1)}, bf16[2,2048,1024]{2,1,0:T(8,128)(2,1)}, u32[]{:S(2)}) copy-start(bf16[2,2048,1024]{2,1,0:T(8,128)(2,1)} %all-gather.10.cloned.1.call-done) | copy-start | bytes 25165828
  397.4 6.0 %collective-permute-start.3 = (bf16[15,1024]{1,0:T(8,128)(2,1)S(1)}, bf16[15,1024]{1,0:T(8,128)(2,1)S(1)}, u32[]{:S(2)}, u32[]{:S(2)}) collective-permute-start(bf16[15,1024]{1,0:T(8,128)(2,1)S(1)} %get-tuple-element.20), channel_id=1, source_target_pairs={{2,0},{4,2},{6,4},{8,6},{10,8},{12,10},{14,12},{16,14},{18,16},{20... | collective-permute-start | bytes 92168 | tf_op jit(solution)/shard_map/ppermute | solution.py:20
  401.4 6.5 %collective-permute-start.2 = (bf16[15,1024]{1,0:T(8,128)(2,1)S(1)}, bf16[15,1024]{1,0:T(8,128)(2,1)S(1)}, u32[]{:S(2)}, u32[]{:S(2)}) collective-permute-start(bf16[15,1024]{1,0:T(8,128)(2,1)S(1)} %get-tuple-element.19), channel_id=1, source_target_pairs={{0,2},{2,4},{4,6},{6,8},{8,10},{10,12},{12,14},{14,16},{16,18},{18... | collective-permute-start | bytes 92168 | tf_op jit(solution)/shard_map/ppermute | solution.py:17
  419.8 11.0 %copy-start.3 = (bf16[384,1024]{1,0:T(8,128)(2,1)S(1)}, bf16[384,1024]{1,0:T(8,128)(2,1)}, u32[]{:S(2)}) copy-start(bf16[384,1024]{1,0:T(8,128)(2,1)} %add_convert_fusion.1) | copy-start | bytes 2359300
Sparse Core Ops, SparseCore 0:
  8.9 11.6 all-gather.7
  23.4 109.8 all-gather.11
  136.0 110.3 all-gather.9
  249.0 110.3 all-gather.15
  360.8 11.5 all-gather.13
  377.9 10.9 all-gather.17
  421.5 9.2 all-gather.19
where the time goes:
time: 444 us; the launch traced here: 443 us
  waiting for transfers between devices  356 us (80%)
  matrix products  26.6 us (6%)
  other arithmetic  23.1 us (5%)
  between operations  13.8 us (3%)
  starting transfers between devices  12.4 us (3%)
  blocking collectives  10.4 us (2%)
    all_gather x1, waiting for transfers between devices, local(): lax.all_gather(gate_weight, 'sp', axis=1, tiled=True)  111 us
    all_gather x1, waiting for transfers between devices, local(): lax.all_gather(a_weight, 'sp', axis=1, tiled=True)  108 us
    all_gather x1, waiting for transfers between devices, local(): lax.all_gather(out_weight, 'sp', axis=1, tiled=True)  81.3 us
    all_gather x2, waiting for transfers between devices, local(): mixed_rows = lax.all_gather(mixed_in, 'tp', axis=1, tiled=True)  22.4 us
    all_gather x2, waiting for transfers between devices, local(): full_rows = lax.all_gather(current, 'tp', axis=1, tiled=True)  22 us
    reduce_sum x2, other arithmetic, local(): jnp.sum(conv_out, axis=1, keepdims=True)  16.1 us
    dot_general x2, matrix products, local(): jnp.dot(mixed_rows, gathered[2][layer_index], preferred_element_type=jnp....  10.7 us
    psum x2, blocking collectives, local(): lax.psum((jnp.sum(conv_out, axis=1, keepdims=True), jnp.sum(conv_out * co...  10.4 us
  transfers between devices with their start and end apart: 11, of which 9 were waited for; matrix products, arithmetic and copies ran while one was open for 5% of the time, Pallas kernels for 0%

commit v1 on v0

--- a/solution.py
+++ b/solution.py
@@ -1,12 +1,137 @@
+import functools
+
 import jax
 import jax.numpy as jnp
 from jax import lax
+from jax.experimental import pallas as pl
+from jax.experimental.pallas import tpu as pltpu
 from jax.sharding import PartitionSpec as P
 
 D = 2048
 
 
 EPSILON = 1e-06
+MESH = pl.DeviceIdType.MESH
+LOOKAHEAD = 3
+ORDERS = ((0, 1, 2), (0, 2, 1), (0, 1, 2), (0, 2, 1), (2, 0, 1), (1, 0, 2))
+
+
+def grid_of(mesh):
+    count = mesh.shape["sp"]
+    row = mesh.devices[:, 0]
+    coords = [getattr(device, "coords", None) for device in row]
+    if any(c is None for c in coords):
+        return (count // 4, 2, 2) if count % 4 == 0 else (count, 1, 1)
+    sizes = tuple(len({c[axis] for c in coords}) for axis in (2, 1, 0))
+    if sizes[0] * sizes[1] * sizes[2] != count:
+        return (count, 1, 1)
+    return sizes
+
+
+def gather_kernel(sizes, halves, pieces, *refs):
+    count = (len(refs) - 3) // 2
+    ins, outs = refs[:count], refs[count : 2 * count]
+    local_sem, send_sem, recv_sem = refs[2 * count :]
+    me = lax.axis_index("sp")
+    strides = (sizes[1] * sizes[2], sizes[2], 1)
+    where = [lax.rem(me // strides[k], sizes[k]) for k in range(3)]
+    half_rows = ins[0].shape[1] // halves
+
+    def peer(axis, step):
+        other = lax.rem(where[axis] + step, sizes[axis])
+        return me + (other - where[axis]) * strides[axis]
+
+    peers = [(axis, step) for axis in range(3) for step in range(1, sizes[axis])]
+    barrier = pltpu.get_barrier_semaphore()
+    for axis, step in peers:
+        pl.semaphore_signal(barrier, inc=1, device_id={"sp": peer(axis, step)}, device_id_type=MESH)
+    pl.semaphore_wait(barrier, len(peers))
+
+    def rows_of(piece):
+        return pl.ds(pieces[piece][2] * half_rows, half_rows)
+
+    def block(piece, done):
+        matrix, layer, _ = pieces[piece]
+        index = [slice(None) if axis in done else where[axis] for axis in range(3)]
+        return outs[matrix].at[(layer, *index, rows_of(piece), slice(None))]
+
+    def local(piece):
+        matrix, layer, _ = pieces[piece]
+        return pltpu.make_async_copy(
+            ins[matrix].at[layer, rows_of(piece), :], block(piece, ()), local_sem.at[piece]
+        )
+
+    def copies(piece, phase):
+        matrix, layer, _ = pieces[piece]
+        order = ORDERS[piece % len(ORDERS)]
+        axis = order[phase]
+        target = block(piece, order[:phase])
+        source = ins[matrix].at[layer, rows_of(piece), :] if phase == 0 else target
+        found = []
+        for step in range(1, sizes[axis]):
+            slot = peers.index((axis, step))
+            found.append(
+                pltpu.make_async_remote_copy(
+                    src_ref=source,
+                    dst_ref=target,
+                    send_sem=send_sem.at[piece, slot],
+                    recv_sem=recv_sem.at[piece, slot],
+                    device_id={"sp": peer(axis, step)},
+                    device_id_type=MESH,
+                )
+            )
+        return found
+
+    def start(piece, phase):
+        if phase == 0:
+            local(piece).start()
+        for copy in copies(piece, phase):
+            copy.start()
+
+    def landed(piece, phase):
+        if phase == 0:
+            local(piece).wait()
+        for copy in copies(piece, phase):
+            copy.wait_recv()
+
+    total = len(pieces)
+    for piece in range(min(LOOKAHEAD, total)):
+        start(piece, 0)
+    for step in range(total + 1):
+        if step + LOOKAHEAD < total:
+            start(step + LOOKAHEAD, 0)
+        if step < total:
+            landed(step, 0)
+            start(step, 1)
+        if step >= 1:
+            landed(step - 1, 1)
+            start(step - 1, 2)
+    for piece in range(total):
+        landed(piece, 2)
+        for phase in range(3):
+            for copy in copies(piece, phase):
+                copy.wait_send()
+
+
+def gather_weights(sizes, weights, pieces, halves):
+    layers, depth, columns = weights[0].shape
+    slots = sum(size - 1 for size in sizes)
+    full = (layers, *sizes, depth, columns)
+    moved = sum(size - 1 for size in sizes)
+    gathered = pl.pallas_call(
+        functools.partial(gather_kernel, sizes, halves, pieces),
+        out_shape=[jax.ShapeDtypeStruct(full, jnp.bfloat16)] * len(weights),
+        in_specs=[pl.BlockSpec(memory_space=pltpu.VMEM)] * len(weights),
+        out_specs=[pl.BlockSpec(memory_space=pl.ANY)] * len(weights),
+        scratch_shapes=[
+            pltpu.SemaphoreType.DMA((len(pieces),)),
+            pltpu.SemaphoreType.DMA((len(pieces), slots)),
+            pltpu.SemaphoreType.DMA((len(pieces), slots)),
+        ],
+        compiler_params=pltpu.CompilerParams(collective_id=0, has_side_effects=True),
+    )(*weights)
+    count = sizes[0] * sizes[1] * sizes[2]
+    return [whole.reshape(layers, count * depth, columns) for whole in gathered]
 
 
 def with_halo(block, sides, width):
@@ -22,6 +147,16 @@
     return block
 
 
+def all_channels(block):
+    if lax.axis_size("tp") != 2:
+        return lax.all_gather(block, "tp", axis=1, tiled=True)
+    other = lax.ppermute(block, "tp", [(0, 1), (1, 0)])
+    first = lax.axis_index("tp") == 0
+    return jnp.concatenate(
+        [jnp.where(first, block, other), jnp.where(first, other, block)], axis=1
+    )
+
+
 def normalize_rows(stream_f, gain):
     factor = lax.rsqrt(jnp.mean(stream_f * stream_f, axis=1, keepdims=True) + EPSILON)
     return (stream_f * factor * gain[None, :]).astype(jnp.bfloat16)
@@ -43,19 +178,31 @@
 
 
 def local(
-    stream, norm_gain, a_weight, gate_weight, conv_weight, conv_bias, ln_gain, ln_shift, out_weight
+    sizes,
+    stream,
+    norm_gain,
+    a_weight,
+    gate_weight,
+    conv_weight,
+    conv_bias,
+    ln_gain,
+    ln_shift,
+    out_weight,
 ):
     reach = (conv_weight.shape[1] - 1) // 2
     layer_total = a_weight.shape[0]
-    gathered = (
-        lax.all_gather(a_weight, "sp", axis=1, tiled=True),
-        lax.all_gather(gate_weight, "sp", axis=1, tiled=True),
-        lax.all_gather(out_weight, "sp", axis=1, tiled=True),
-    )
+    halves = 2
+    pieces = [
+        (matrix, layer, half)
+        for layer in range(layer_total)
+        for matrix in range(3)
+        for half in range(halves)
+    ]
+    gathered = gather_weights(sizes, (a_weight, gate_weight, out_weight), pieces, halves)
     current = stream
     for layer_index in range(layer_total):
         stream_f = current.astype(jnp.float32)
-        full_rows = lax.all_gather(current, "tp", axis=1, tiled=True)
+        full_rows = all_channels(current)
         normed = normalize_rows(full_rows.astype(jnp.float32), norm_gain[layer_index])
         linear = jnp.dot(normed, gathered[0][layer_index], preferred_element_type=jnp.float32)
         gating = jnp.dot(normed, gathered[1][layer_index], preferred_element_type=jnp.float32)
@@ -74,7 +221,7 @@
         mixed_in = finish_norm(
             conv_out, row_sum, row_squares, ln_gain[layer_index], ln_shift[layer_index]
         )
-        mixed_rows = lax.all_gather(mixed_in, "tp", axis=1, tiled=True)
+        mixed_rows = all_channels(mixed_in)
         branch = jnp.dot(mixed_rows, gathered[2][layer_index], preferred_element_type=jnp.float32)
         current = (stream_f + branch).astype(jnp.bfloat16)
     return current
@@ -93,5 +240,9 @@
         P(None, "sp", "tp"),
     )
     return jax.shard_map(
-        local, mesh=mesh, in_specs=placed, out_specs=P("sp", "tp"), check_vma=False
+        functools.partial(local, grid_of(mesh)),
+        mesh=mesh,
+        in_specs=placed,
+        out_specs=P("sp", "tp"),
+        check_vma=False,
     )

time: 444 us -> 341 us (0.77)
  waiting for transfers between devices: 356 us -> 9.22 us
  Pallas kernels: 0 us -> 254 us
  local copies, waits for them, and re-layouts: 0.8 us -> 22.9 us
  matrix products: 26.6 us -> 12.2 us
  between operations: 13.8 us -> 0.28 us
    all_gather x7 -> x0, waiting for transfers between devices: 344 us -> none  [the longest x1 111 us: local(): lax.all_gather(gate_weight, 'sp', axis=1, tiled=True)]
    pallas_call x0 -> x1, Pallas kernels: none -> 254 us  [gather_weights(): pl.pallas_call(functools.partial(gather_kernel, sizes, halves, pieces), o...]
    slice x0 -> x2, local copies, waits for them, and re-layouts: none -> 14.8 us  [the longest x1 9.57 us: local(): gathered[0][layer_index]]
    dot_general x2, matrix products: 10.7 us -> 4.55 us  [local(): jnp.dot(mixed_rows, gathered[2][layer_index], preferred_element_type=jnp....]
    dot_general x2, matrix products: 9.44 us -> 3.75 us  [local(): jnp.dot(normed, gathered[1][layer_index], preferred_element_type=jnp.floa...]
  transfers between devices with their start and end apart: 11 -> 8, of which waited for: 9 -> 4; matrix products, arithmetic and copies ran while one was open for 5% -> 6% of each run, Pallas kernels for 0% -> 75%
where the time goes in v1:
time: 341 us; the launch traced here: 340 us
  Pallas kernels  254 us (74%)
  local copies, waits for them, and re-layouts  22.9 us (7%)
  other arithmetic  20.1 us (6%)
  starting transfers between devices  12.3 us (4%)
  matrix products  12.2 us (4%)
  waiting for transfers between devices  9.22 us (3%)
  blocking collectives  9.18 us (3%)
    pallas_call x1, Pallas kernels, gather_weights(): pl.pallas_call(functools.partial(gather_kernel, sizes, halves, pieces), o...  254 us
    reduce_sum x2, other arithmetic, local(): jnp.sum(conv_out, axis=1, keepdims=True)  16.1 us
    slice x1, local copies, waits for them, and re-layouts, local(): gathered[0][layer_index]  9.57 us
    psum x2, blocking collectives, local(): lax.psum((jnp.sum(conv_out, axis=1, keepdims=True), jnp.sum(conv_out * co...  9.18 us
  transfers between devices with their start and end apart: 8, of which 4 were waited for; matrix products, arithmetic and copies ran while one was open for 6% of the time, Pallas kernels for 75%

profile of v1, /device:TPU:9, one launch (start us, length us, event | category | flops | bytes accessed | tf_op | source)
XLA Modules:
  0.0 340.2 jit_solution(9048391082259242725)
XLA Ops:
  0.7 0.9 fusion.90
  5.8 254.0 %shard_map.91 = (bf16[2,4,2,2,128,1024]{5,4,3,2,1,0:T(8,128)(2,1)}, bf16[2,4,2,2,128,1024]{5,4,3,2,1,0:T(8,128)(2,1)}, bf16[2,4,2,2,128,1024]{5,4,3,2,1,0:T(8,128)(2,1)}) custom-call(bf16[2,128,1024]{2,1,0:T(8,128)(2,1)} %refs_0_.1, bf16[2,128,1024]{2,1,0:T(8,128)(2,1)} %refs_1_.1, bf16[2,128,1024]{2,1,0:T(8,128)(2,1)} %refs_2_.1), custom_call_target="tpu_custom_call" | custom-call | tf_op jit(solution)/shard_map/pallas_call | solution.py:121
  259.8 9.6 %fusion.84 = (bf16[1,4,2,2,128,1024]{5,4,3,2,1,0:T(8,128)(2,1)}, bf16[1,4,2,2,128,1024]{5,4,3,2,1,0:T(8,128)(2,1)S(1)}, bf16[1,4,2,2,128,1024]{5,4,3,2,1,0:T(8,128)(2,1)S(1)}, bf16[1,4,2,2,128,1024]{5,4,3,2,1,0:T(8,128)(2,1)}) fusion(bf16[2,4,2,2,128,1024]{5,4,3,2,1,0:T(8,128)(2,1)} %get-tuple-element.8, bf16[2,4,2,2,128,1024]{5,4,3,2,1,0:T(8,128)(2,1)} %get-tuple-element.9), kind=kLoop, calls=%fused_computation.200 | loop fusion | bytes 33554432 | tf_op jit(solution)/shard_map/slice | solution.py:207
  269.9 1.9 fusion.79
  271.8 2.0 multiply_convert_fusion.3
  273.8 1.9 collective-permute-start.2
  275.8 3.4 collective-permute-start.1
  279.2 3.0 collective-permute-done.1
  282.2 8.0 %fusion.83 = (f32[384]{0:T(512)S(1)}, f32[384]{0:T(512)S(1)}, f32[384,1024]{1,0:T(8,128)S(1)}) fusion(f32[1024]{0:T(1024)S(1)} %bitcast.108, bf16[15,1024]{1,0:T(8,128)(2,1)S(1)} %collective-permute-done.2, bf16[384,1024]{1,0:T(8,128)(2,1)S(1)} %multiply_convert_fusion.3, f32[1024]{0:T(1024)S(1)} %bitcast.109, f32[1024]{0:T(1024)S(1)} %bitcast.110, ...), kind=kLoop, calls=%fused_computation.199 | loop fusion | flops 73137408 | bytes 2554880 | tf_op jit(solution)/shard_map/reduce_sum | solution.py:216
  290.3 5.7 %all-reduce.1 = (f32[384,1]{0,1:T(1,128)S(1)}, f32[384,1]{0,1:T(1,128)S(1)}) all-reduce(f32[384,1]{0,1:T(1,128)S(1)} %broadcast_in_dim.14, f32[384,1]{0,1:T(1,128)S(1)} %broadcast_in_dim.15), channel_id=1, replica_groups=mesh['sp'=16,'tp'=2] {'tp'}, use_global_device_ids=true, to_apply=%region_2.3 | all-reduce | flops 768 | bytes 6144 | tf_op jit(solution)/shard_map/psum | solution.py:214
  297.1 5.3 %fusion.86 = (bf16[1,4,2,2,128,1024]{5,4,3,2,1,0:T(8,128)(2,1)}, bf16[1,4,2,2,128,1024]{5,4,3,2,1,0:T(8,128)(2,1)S(1)}) fusion(bf16[2,4,2,2,128,1024]{5,4,3,2,1,0:T(8,128)(2,1)} %get-tuple-element.10), kind=kLoop, calls=%fused_computation.202 | loop fusion | bytes 16777216 | tf_op jit(solution)/shard_map/slice | solution.py:225
  303.2 1.8 add_convert_fusion.1
  305.3 2.1 collective-permute-done.4
  307.9 1.7 copy-done.2
  309.6 1.9 fusion.76
  311.8 2.0 multiply_convert_fusion.1
  313.8 1.9 collective-permute-start.6
  315.7 3.4 collective-permute-start.5
  319.1 1.0 fusion.89
  320.1 2.1 collective-permute-done.5
  322.2 8.1 %fusion.82 = (f32[384]{0:T(512)S(1)}, f32[384]{0:T(512)S(1)}, f32[384,1024]{1,0:T(8,128)S(1)}) fusion(f32[1024]{0:T(1024)S(1)} %bitcast.107, bf16[15,1024]{1,0:T(8,128)(2,1)S(1)} %collective-permute-done.6, bf16[384,1024]{1,0:T(8,128)(2,1)S(1)} %multiply_convert_fusion.1, f32[1024]{0:T(1024)S(1)} %bitcast.106, f32[1024]{0:T(1024)S(1)} %bitcast.140, ...), kind=kLoop, calls=%fused_computation.198 | loop fusion | flops 73137408 | bytes 2554880 | tf_op jit(solution)/shard_map/reduce_sum | solution.py:216
  330.2 3.4 %all-reduce = (f32[384,1]{0,1:T(1,128)S(1)}, f32[384,1]{0,1:T(1,128)S(1)}) all-reduce(f32[384,1]{0,1:T(1,128)S(1)} %broadcast_in_dim.16, f32[384,1]{0,1:T(1,128)S(1)} %broadcast_in_dim.17), channel_id=1, replica_groups=mesh['sp'=16,'tp'=2] {'tp'}, use_global_device_ids=true, to_apply=%region_7.8 | all-reduce | flops 768 | bytes 6144 | tf_op jit(solution)/shard_map/psum | solution.py:214
  334.7 1.9 collective-permute-done.7
  337.5 2.7 add_convert_fusion
  (41 shorter events, 10.2 us)
Async XLA Ops:
  0.0 269.4 %collective-permute-start = (bf16[384,1024]{1,0:T(8,128)(2,1)}, bf16[384,1024]{1,0:T(8,128)(2,1)S(1)}, u32[]{:S(2)}, u32[]{:S(2)}) collective-permute-start(bf16[384,1024]{1,0:T(8,128)(2,1)} %param.9), channel_id=1, source_target_pairs={{0,1},{1,0},{2,3},{3,2},{4,5},{5,4},{6,7},{7,6},{8,9},{9,8},{10,11... | collective-permute-start | bytes 2359304 | tf_op jit(solution)/shard_map/ppermute | solution.py:153
  259.8 9.6 %copy-start.3 = (bf16[384,1024]{1,0:T(8,128)(2,1)S(1)}, bf16[384,1024]{1,0:T(8,128)(2,1)}, u32[]{:S(2)}) copy-start(bf16[384,1024]{1,0:T(8,128)(2,1)} %param.9) | copy-start | bytes 2359300
  271.8 7.3 %copy-start.4 = (f32[2,1024]{1,0:T(2,128)S(1)}, f32[2,1024]{1,0:T(2,128)}, u32[]{:S(2)}) copy-start(f32[2,1024]{1,0:T(2,128)} %param.15) | copy-start | bytes 24580
  273.8 5.3 %collective-permute-start.2 = (bf16[15,1024]{1,0:T(8,128)(2,1)S(1)}, bf16[15,1024]{1,0:T(8,128)(2,1)S(1)}, u32[]{:S(2)}, u32[]{:S(2)}) collective-permute-start(bf16[15,1024]{1,0:T(8,128)(2,1)S(1)} %get-tuple-element.42), channel_id=1, source_target_pairs={{2,0},{4,2},{6,4},{8,6},{10,8},{12,10},{14,12},{16,14},{18,16},{20... | collective-permute-start | bytes 92168 | tf_op jit(solution)/shard_map/ppermute | solution.py:145
  275.8 6.5 %collective-permute-start.1 = (bf16[15,1024]{1,0:T(8,128)(2,1)S(1)}, bf16[15,1024]{1,0:T(8,128)(2,1)S(1)}, u32[]{:S(2)}, u32[]{:S(2)}) collective-permute-start(bf16[15,1024]{1,0:T(8,128)(2,1)S(1)} %get-tuple-element.41), channel_id=1, source_target_pairs={{0,2},{2,4},{4,6},{6,8},{8,10},{10,12},{12,14},{14,16},{16,18},{18... | collective-permute-start | bytes 92168 | tf_op jit(solution)/shard_map/ppermute | solution.py:142
  296.7 5.7 %collective-permute-start.3 = (bf16[384,1024]{1,0:T(8,128)(2,1)S(1)}, bf16[384,1024]{1,0:T(8,128)(2,1)S(1)}, u32[]{:S(2)}, u32[]{:S(2)}) collective-permute-start(bf16[384,1024]{1,0:T(8,128)(2,1)S(1)} %multiply_convert_fusion.2), channel_id=1, source_target_pairs={{0,1},{1,0},{2,3},{3,2},{4,5},{5,4},{6,7},{7,6},{8,9},{9,8},{10,11... | collective-permute-start | bytes 2359304 | tf_op jit(solution)/shard_map/ppermute | solution.py:153
  305.1 2.4 collective-permute-start.4
  307.4 2.2 copy-start.2
  309.6 2.2 copy-start.1
  313.8 6.3 %collective-permute-start.6 = (bf16[15,1024]{1,0:T(8,128)(2,1)S(1)}, bf16[15,1024]{1,0:T(8,128)(2,1)S(1)}, u32[]{:S(2)}, u32[]{:S(2)}) collective-permute-start(bf16[15,1024]{1,0:T(8,128)(2,1)S(1)} %get-tuple-element.40), channel_id=1, source_target_pairs={{2,0},{4,2},{6,4},{8,6},{10,8},{12,10},{14,12},{16,14},{18,16},{20... | collective-permute-start | bytes 92168 | tf_op jit(solution)/shard_map/ppermute | solution.py:145
  315.7 6.5 %collective-permute-start.5 = (bf16[15,1024]{1,0:T(8,128)(2,1)S(1)}, bf16[15,1024]{1,0:T(8,128)(2,1)S(1)}, u32[]{:S(2)}, u32[]{:S(2)}) collective-permute-start(bf16[15,1024]{1,0:T(8,128)(2,1)S(1)} %get-tuple-element.39), channel_id=1, source_target_pairs={{0,2},{2,4},{4,6},{6,8},{8,10},{10,12},{12,14},{14,16},{16,18},{18... | collective-permute-start | bytes 92168 | tf_op jit(solution)/shard_map/ppermute | solution.py:142
  333.7 3.8 %copy-start = (bf16[1,4,2,2,128,1024]{5,4,3,2,1,0:T(8,128)(2,1)S(1)}, bf16[1,4,2,2,128,1024]{5,4,3,2,1,0:T(8,128)(2,1)}, u32[]{:S(2)}) copy-start(bf16[1,4,2,2,128,1024]{5,4,3,2,1,0:T(8,128)(2,1)} %get-tuple-element.29) | copy-start | bytes 12582916
  334.3 2.4 collective-permute-start.7
